TPU v7x, 256 devices: a whole 4x4x8 slice. The times are simulated.
256 devices in a mesh: sp: 64 (over z, x, core), tp: 4 (over y).
Axes of the slice: x: 4, y: 4, z: 8, core: 2. Of those that a mesh axis runs over, the one named last changes fastest.
Arguments:
- queries: bfloat16 [8192, 2048], P('sp', 'tp'), may hold values from -6 to 6
- keys: bfloat16 [8192, 512], P('sp', 'tp'), may hold values from -6 to 6
- values: bfloat16 [8192, 512], P('sp', 'tp'), may hold values from -6 to 6
- break_bias: float32 [16], P('tp'), as said below
- residual: bfloat16 [8192, 4096], P(('sp', 'tp')), may hold values from -6 to 6
- w_out: bfloat16 [2048, 4096], P('tp'), may hold values from -0.125 to 0.125
- ffn_gain: float32 [4096], replicated, may hold values from 0.1 to 1.9
- pick_ids: int32 [8192, 2], P('sp'), may hold values from 0 to 63, as said below
- pair_logit: float32 [8192], P('sp'), may hold values from -8 to 8
- w_gate: bfloat16 [64, 4096, 1024], P('sp', None, 'tp'), may hold values from -0.09375 to 0.09375
- w_up: bfloat16 [64, 4096, 1024], P('sp', None, 'tp'), may hold values from -0.09375 to 0.09375
- w_down: bfloat16 [64, 1024, 4096], P('sp', 'tp'), may hold values from -0.1875 to 0.1875
- out_gain: float32 [4096], replicated, may hold values from 0.1 to 1.9
Outputs:
- new_stream: bfloat16 [8192, 4096], P(('sp', 'tp'))
Inputs may be any that keep to these rules, and one draw needn't show every extreme that they name: `break_bias`: the logarithm of a break rate per position: between ln(0.02 / 8192) and ln(8 / 128). `pick_ids`: A row's 2 experts differ and lie in one group of 16 consecutive experts. In each aligned block of 32 rows no expert is named more than 2 times, and some expert exactly 2 times.
All inputs are finite; a program needn't handle non-finite values.
Results may differ from a plain program's by a relative error of at most 0.017.
Values may be sent and summed in bfloat16 or wider, within the bound.
No kernel may reach another device: no remote copies, remote signals or barrier semaphores. Data moves between devices by JAX's collectives and lax.ppermute only.
A program may use at most 64 MiB of HBM per device.

v0:
```python
import jax
import jax.numpy as jnp
from jax import lax
from jax.sharding import PartitionSpec as P

HEAD = 128
TOP = 2


epsilon = 1e-06


def sent_together(arrays, axis, dim, along):
    widths = [a.shape[along] for a in arrays]
    both = jnp.concatenate(arrays, axis=along)
    out = lax.all_gather(both, axis, axis=dim, tiled=True)
    return tuple(jnp.split(out, [sum(widths[:k]) for k in range(1, len(widths))], axis=along))


def split_up(shard, dim, peers):
    before, after = (shard.shape[:dim], shard.shape[dim + 1 :])
    return jnp.moveaxis(shard.reshape(*before, peers, -1, *after), dim, 0)


def summed_on_arrival(shard, axis, dim):
    parts = split_up(shard, dim, lax.axis_size(axis))
    arrived = lax.all_to_all(parts, axis, split_axis=0, concat_axis=0, tiled=True)
    return arrived.astype(jnp.float32).sum(axis=0)


def stick_block(carried, query_rows, key_block, value_block, head_bias, query_pos, key_pos):
    output, used_up = carried
    scores = jnp.einsum("qcgd,scd->qcgs", query_rows, key_block, preferred_element_type=jnp.float32)
    scores = scores * query_rows.shape[-1] ** (-0.5) + head_bias[None, :, :, None]
    before = ((key_pos[None, :] < query_pos[:, None]) & True)[:, None, None, :]
    breaks = jnp.where(before, jax.nn.softplus(scores), 0.0)
    behind = lax.cumsum(breaks, axis=3, reverse=True) - breaks
    weights = jnp.where(
        before, jnp.exp(jax.nn.log_sigmoid(scores) - behind - used_up[..., None]), 0.0
    )
    output = output + jnp.einsum(
        "qcgs,scd->qcgd",
        weights.astype(jnp.bfloat16),
        value_block,
        preferred_element_type=jnp.float32,
    )
    return (output, used_up + jnp.sum(breaks, axis=3))


def attend_all(query_rows, query_pos, key_all, value_all, head_bias):
    count, kv_local, per_key, _ = query_rows.shape
    extent = key_all.shape[0]
    window = min(512, extent)
    needed = (query_pos[count - 1] + window) // window
    initial = (
        jnp.zeros((count, kv_local, per_key, HEAD), jnp.float32),
        jnp.zeros((count, kv_local, per_key), jnp.float32),
    )

    def visit(step_index, carried):
        first_key = (needed - 1 - step_index) * window
        key_block = lax.dynamic_slice_in_dim(key_all, first_key, window, 0).reshape(
            window, kv_local, HEAD
        )
        value_block = lax.dynamic_slice_in_dim(value_all, first_key, window, 0).reshape(
            window, kv_local, HEAD
        )
        key_pos = first_key + jnp.arange(window, dtype=jnp.int32)
        return stick_block(
            carried, query_rows, key_block, value_block, head_bias, query_pos, key_pos
        )

    return lax.fori_loop(0, needed, visit, initial)[0]


def normed_heads(output):
    scaled = output * lax.rsqrt(jnp.mean(output * output, axis=-1, keepdims=True) + epsilon)
    return scaled.astype(jnp.bfloat16).reshape(output.shape[0], -1)


def on_device(
    queries,
    keys,
    values,
    break_bias,
    residual,
    w_out,
    ffn_gain,
    pick_ids,
    pair_logit,
    w_gate,
    w_up,
    w_down,
    out_gain,
):
    length = queries.shape[0]
    kv_local = keys.shape[1] // HEAD
    per_key = queries.shape[1] // keys.shape[1]
    query_rows = queries.reshape(length, kv_local, per_key, HEAD)
    head_bias = break_bias.reshape(kv_local, per_key)
    position = lax.axis_index("sp")
    offset = position * length
    query_pos = offset + jnp.arange(length, dtype=jnp.int32)
    key_all, value_all = sent_together((keys, values), "sp", 0, 1)
    head_out = normed_heads(attend_all(query_rows, query_pos, key_all, value_all, head_bias))
    quarters = lax.axis_size("tp")
    quarter = lax.axis_index("tp")
    slice_rows = length // quarters
    width = w_out.shape[1]
    experts = lax.axis_size("sp")
    capacity = max(2, (3 * slice_rows + experts - 1) // experts)
    mixed = summed_on_arrival(
        jnp.dot(head_out, w_out, preferred_element_type=jnp.float32).astype(jnp.bfloat16), "tp", 0
    )
    stream = (residual.astype(jnp.float32) + mixed).astype(jnp.bfloat16)
    routed = lax.dynamic_slice_in_dim(pick_ids, quarter * slice_rows, slice_rows, 0)[None]
    stream_float = stream.astype(jnp.float32)
    ffn_in = (
        stream_float
        * lax.rsqrt(jnp.mean(stream_float * stream_float, axis=-1, keepdims=True) + epsilon)
        * ffn_gain
    ).astype(jnp.bfloat16)
    blocks = routed.shape[0]
    entries = ffn_in.reshape(blocks, slice_rows, width)
    flat_ids = routed.reshape(blocks, slice_rows * TOP)
    places = jnp.arange(slice_rows * TOP, dtype=jnp.int32)
    earlier = places[None, :] < places[:, None]
    matches = (flat_ids[:, :, None] == flat_ids[:, None, :]) & earlier[None]
    ranks = jnp.sum(matches.astype(jnp.int32), axis=2)
    targets = (flat_ids * capacity + ranks).reshape(blocks, slice_rows, TOP)
    block_ids = jnp.arange(blocks, dtype=jnp.int32)[:, None]
    outgoing = jnp.zeros((blocks, experts * capacity, width), jnp.bfloat16)
    for pick_index in range(TOP):
        outgoing = outgoing.at[block_ids, targets[:, :, pick_index]].set(entries)
    arrived = lax.all_to_all(outgoing, "sp", split_axis=1, concat_axis=1, tiled=True).reshape(
        -1, width
    )
    piece = lax.all_gather(arrived, "tp", axis=0, tiled=True)
    gated = jax.nn.silu(jnp.dot(piece, w_gate[0], preferred_element_type=jnp.float32))
    hidden = (gated * jnp.dot(piece, w_up[0], preferred_element_type=jnp.float32)).astype(
        jnp.bfloat16
    )
    results = summed_on_arrival(
        jnp.dot(hidden, w_down[0], preferred_element_type=jnp.float32).astype(jnp.bfloat16), "tp", 0
    ).astype(jnp.bfloat16)
    returned = lax.all_to_all(results, "sp", split_axis=0, concat_axis=0, tiled=True)
    own_targets = targets[0]
    logits = lax.dynamic_slice_in_dim(pair_logit, quarter * slice_rows, slice_rows, 0)
    leading = returned[own_targets[:, 0]].astype(jnp.float32)
    trailing = returned[own_targets[:, 1]].astype(jnp.float32)
    blended = (
        jax.nn.sigmoid(logits)[:, None] * leading + jax.nn.sigmoid(-logits)[:, None] * trailing
    )
    blend_scale = lax.rsqrt(jnp.mean(blended * blended, axis=-1, keepdims=True) + epsilon)
    return (stream_float + blended * blend_scale * out_gain).astype(jnp.bfloat16)


def solution(mesh):
    placed = (
        P("sp", "tp"),
        P("sp", "tp"),
        P("sp", "tp"),
        P("tp"),
        P(("sp", "tp"), None),
        P("tp", None),
        P(),
        P("sp", None),
        P("sp"),
        P("sp", None, "tp"),
        P("sp", None, "tp"),
        P("sp", "tp", None),
        P(),
    )
    return jax.shard_map(
        on_device, mesh=mesh, in_specs=placed, out_specs=P(("sp", "tp"), None), check_vma=False
    )
```

profile of v0, /device:TPU:1, one launch (start us, length us, event | category | flops | bytes accessed | tf_op | source)
XLA Modules:
  0.0 566.2 jit_solution(12902938467212862782)
XLA Ops:
  6.5 1.6 pad_maximum_fusion
  12.6 80.7 %all-gather.4.cloned.1.call-done = bf16[8192,256]{1,0:T(8,128)(2,1)} async-done(((bf16[128,256]{1,0:T(8,128)(2,1)}), bf16[8192,256]{1,0:T(8,128)(2,1)}) %all-gather.4.cloned.1.call-update) | async-done | bytes 4194320 | tf_op jit(solution)/shard_map/all_gather | solution.py:16
  93.3 4.5 fusion.65
  97.8 13.4 %while.15 = (s32[]{:T(128)}, f32[128,1,4,128]{0,3,2,1:T(8,128)S(1)}, f32[128,1,4]{0,2,1:T(4,128)S(1)}, s32[]{:T(128)}, s32[]{:T(128)}, /*index=5*/bf16[8192,128]...) while((s32[]{:T(128)}, ...), condition=%wide.region_4.5_spmd.clone, body=%wide.region_0.4_spmd.clone.sunk | while | flops 175775872 | bytes 12723443 | solution.py:73
  98.0 2.8 fusion.80
  100.8 5.9 %fusion.81 = f32[128,1,4,4,128]{0,3,2,1,4:T(4,128)S(1)} fusion(f32[128,1,4,4,128]{0,4,3,2,1:T(8,128)S(1)} %bitcast.116), kind=kOutput, calls=%fused_computation.22.clone.1 | output fusion | flops 33292288 | bytes 2097152 | tf_op jit(solution)/shard_map/reduce-window.4
  107.2 2.8 fusion.82
  111.2 3.9 convolution_convert_fusion.1
  115.2 4.1 all-to-all-start
  119.9 14.0 %all-to-all-done = bf16[4,32,4096]{2,1,0:T(8,128)(2,1)S(1)} async-done(((bf16[4,32,4096]{2,1,0:T(8,128)(2,1)}), bf16[4,32,4096]{2,1,0:T(8,128)(2,1)S(1)}, u32[]{:S(2)}, u32[]{:S(2)}) %all-to-all-start) | async-done | bytes 1048608 | tf_op jit(solution)/shard_map/all_to_all | solution.py:27
  136.7 1.6 scatter_custom_fusion.1
  138.3 3.7 copy.86
  142.6 8.4 %reduce.14 = bf16[128,4096]{1,0:T(8,128)(2,1)S(1)} reduce(bf16[128,1,4096]{2,1,0:T(2,128)(2,1)} %bitcast.118, bf16[]{:T(256)} %broadcast.228), dimensions={1}, to_apply=%bitcast.88.reduce_sub_computation | reduce | bytes 2097154
  152.5 234.5 %all_to_all.27 = bf16[64,2,4096]{2,1,0:T(2,128)(2,1)S(1)} all-to-all(bf16[64,2,4096]{2,1,0:T(2,128)(2,1)} %reshape.352), channel_id=1, replica_groups=mesh['sp'=64,'tp'=4] {'sp'}, dimensions={0} | all-to-all | bytes 2097152 | tf_op jit(solution)/shard_map/all_to_all | solution.py:135
  387.0 3.5 reshape.353
  390.4 3.7 copy.75
  394.2 45.8 %all-gather.6.cloned.1.call-done = bf16[1,512,4096]{2,1,0:T(8,128)(2,1)} async-done(((bf16[1,128,4096]{2,1,0:T(8,128)(2,1)}), bf16[1,512,4096]{2,1,0:T(8,128)(2,1)}) %all-gather.6.cloned.1.call-update) | async-done | bytes 4194320 | tf_op jit(solution)/shard_map/all_gather | solution.py:138
  440.0 4.1 fusion.27
  444.1 9.3 %convolution_convert_fusion = bf16[512,4096]{1,0:T(8,128)(2,1)} fusion(bf16[1,256,4096]{2,1,0:T(8,128)(2,1)S(1)} %copy-done, bf16[1,4096,256]{2,1,0:T(8,128)(2,1)} %param.25, bf16[1,512,4096]{2,1,0:T(8,128)(2,1)} %all-gather.6.cloned.1.call-done, f32[512,256]{1,0:T(8,128)S(1)} %fusion.27), kind=kOutput, calls=%fused_computation.39 | convolution fusion | flops 2150367232 | bytes 13107200 | tf_op jit(solution)/shard_map/dot_general | solution.py:144
  453.4 53.5 %all_to_all.28 = bf16[4,128,4096]{2,1,0:T(8,128)(2,1)} all-to-all(bf16[4,128,4096]{2,1,0:T(8,128)(2,1)} %bitcast.120), channel_id=1, replica_groups=mesh['sp'=64,'tp'=4] {'tp'}, dimensions={0} | all-to-all | bytes 8388608 | tf_op jit(solution)/shard_map/all_to_all | solution.py:27
  507.0 3.1 reduce_sum.75
  511.6 12.1 %all-to-all-start.3 = ((bf16[64,2,4096]{2,1,0:T(2,128)(2,1)}), bf16[64,2,4096]{2,1,0:T(2,128)(2,1)}, u32[]{:S(2)}, u32[]{:S(2)}) async-start(bf16[64,2,4096]{2,1,0:T(2,128)(2,1)} %all_to_all.20), calls=%async_computation.3 | async-start | bytes 2097152 | tf_op jit(solution)/shard_map/all_to_all | solution.py:146
  524.0 27.8 %all-to-all-done.3 = bf16[64,2,4096]{2,1,0:T(2,128)(2,1)} async-done(((bf16[64,2,4096]{2,1,0:T(2,128)(2,1)}), bf16[64,2,4096]{2,1,0:T(2,128)(2,1)}, u32[]{:S(2)}, u32[]{:S(2)}) %all-to-all-start.3) | async-done | bytes 1048608 | tf_op jit(solution)/shard_map/all_to_all | solution.py:146
  557.4 2.0 fusion.49
  (65 shorter events, 18.4 us)
Async XLA Ops:
  6.5 437.6 %copy-start = (bf16[1,256,4096]{2,1,0:T(8,128)(2,1)S(1)}, bf16[1,256,4096]{2,1,0:T(8,128)(2,1)}, u32[]{:S(2)}) copy-start(bf16[1,256,4096]{2,1,0:T(8,128)(2,1)} %param.26) | copy-start | bytes 6291460
  6.5 86.8 %all-gather.4.cloned.1.call-start = ((), (), s32[]{:S(2)}) async-start(), calls=%async_computation.4 | async-start | bytes 4259840 | tf_op jit(solution)/shard_map/all_gather | solution.py:16
  12.6 85.2 %copy-start.4 = (f32[4]{0:T(128)S(1)}, f32[4]{0:T(128)}, u32[]{:S(2)}) copy-start(f32[4]{0:T(128)} %param.18) | copy-start | bytes 52
  115.2 20.1 %copy-start.1 = (f32[4096]{0:T(1024)S(1)}, f32[4096]{0:T(1024)}, u32[]{:S(2)}) copy-start(f32[4096]{0:T(1024)} %param.21) | copy-start | bytes 49156
  115.2 18.8 %all-to-all-start = ((bf16[4,32,4096]{2,1,0:T(8,128)(2,1)}), bf16[4,32,4096]{2,1,0:T(8,128)(2,1)S(1)}, u32[]{:S(2)}, u32[]{:S(2)}) async-start(bf16[4,32,4096]{2,1,0:T(8,128)(2,1)} %bitcast.121), calls=%async_computation | async-start | bytes 2097152 | tf_op jit(solution)/shard_map/all_to_all | solution.py:27
  119.3 320.7 %all-gather.6.cloned.1.call-start = ((), (), s32[]{:S(2)}) async-start(), calls=%async_computation.5 | async-start | bytes 5242880 | tf_op jit(solution)/shard_map/all_gather | solution.py:138
  510.0 13.6 %copy-start.3 = (f32[128]{0:T(128)S(1)}, f32[128]{0:T(128)}, u32[]{:S(2)}) copy-start(f32[128]{0:T(128)} %param.23) | copy-start | bytes 1540
  511.6 40.2 %all-to-all-start.3 = ((bf16[64,2,4096]{2,1,0:T(2,128)(2,1)}), bf16[64,2,4096]{2,1,0:T(2,128)(2,1)}, u32[]{:S(2)}, u32[]{:S(2)}) async-start(bf16[64,2,4096]{2,1,0:T(2,128)(2,1)} %all_to_all.20), calls=%async_computation.3 | async-start | bytes 2097152 | tf_op jit(solution)/shard_map/all_to_all | solution.py:146
  553.2 4.2 copy-start.2
Sparse Core Ops, SparseCore 0:
  10.1 83.1 all-gather.3
  394.3 45.6 all-gather.5
where the time goes:
time: 568 us; the launch traced here: 566 us
  blocking collectives  288 us (51%)
  waiting for transfers between devices  168 us (30%)
  other arithmetic  30.3 us (5%)
  local copies, waits for them, and re-layouts  27.5 us (5%)
  matrix products  21.4 us (4%)
  starting transfers between devices  16.2 us (3%)
  between operations  14.3 us (3%)
    all_to_all x1, blocking collectives, on_device(): lax.all_to_all(outgoing, 'sp', split_axis=1, concat_axis=1, tiled=True)  235 us
    all_gather x1, waiting for transfers between devices, sent_together(): out = lax.all_gather(both, axis, axis=dim, tiled=True)  80.7 us
    all_to_all x1, blocking collectives, summed_on_arrival(): lax.all_to_all(parts, axis, split_axis=0, concat_axis=0, tiled=True)  53.5 us
    all_gather x1, waiting for transfers between devices, on_device(): piece = lax.all_gather(arrived, 'tp', axis=0, tiled=True)  45.8 us
    all_to_all x1, waiting for transfers between devices, on_device(): lax.all_to_all(results, 'sp', split_axis=0, concat_axis=0, tiled=True)  27.8 us
    all_to_all x1, waiting for transfers between devices, summed_on_arrival(): lax.all_to_all(parts, axis, split_axis=0, concat_axis=0, tiled=True)  14 us
    all_to_all x1, starting transfers between devices, on_device(): lax.all_to_all(results, 'sp', split_axis=0, concat_axis=0, tiled=True)  12.1 us
  transfers between devices with their start and end apart: 4, of which 4 were waited for; matrix products, arithmetic and copies ran while one was open for 1% of the time, Pallas kernels for 0%

commit v1 on v0

--- a/solution.py
+++ b/solution.py
@@ -1,6 +1,8 @@
 import jax
 import jax.numpy as jnp
 from jax import lax
+from jax.experimental import pallas as pl
+from jax.experimental.pallas import tpu as pltpu
 from jax.sharding import PartitionSpec as P
 
 HEAD = 128
@@ -8,13 +10,6 @@
 
 
 epsilon = 1e-06
-
-
-def sent_together(arrays, axis, dim, along):
-    widths = [a.shape[along] for a in arrays]
-    both = jnp.concatenate(arrays, axis=along)
-    out = lax.all_gather(both, axis, axis=dim, tiled=True)
-    return tuple(jnp.split(out, [sum(widths[:k]) for k in range(1, len(widths))], axis=along))
 
 
 def split_up(shard, dim, peers):
@@ -28,54 +23,98 @@
     return arrived.astype(jnp.float32).sum(axis=0)
 
 
-def stick_block(carried, query_rows, key_block, value_block, head_bias, query_pos, key_pos):
-    output, used_up = carried
-    scores = jnp.einsum("qcgd,scd->qcgs", query_rows, key_block, preferred_element_type=jnp.float32)
-    scores = scores * query_rows.shape[-1] ** (-0.5) + head_bias[None, :, :, None]
-    before = ((key_pos[None, :] < query_pos[:, None]) & True)[:, None, None, :]
-    breaks = jnp.where(before, jax.nn.softplus(scores), 0.0)
-    behind = lax.cumsum(breaks, axis=3, reverse=True) - breaks
-    weights = jnp.where(
-        before, jnp.exp(jax.nn.log_sigmoid(scores) - behind - used_up[..., None]), 0.0
-    )
-    output = output + jnp.einsum(
-        "qcgs,scd->qcgd",
-        weights.astype(jnp.bfloat16),
-        value_block,
-        preferred_element_type=jnp.float32,
-    )
-    return (output, used_up + jnp.sum(breaks, axis=3))
-
-
-def attend_all(query_rows, query_pos, key_all, value_all, head_bias):
-    count, kv_local, per_key, _ = query_rows.shape
-    extent = key_all.shape[0]
-    window = min(512, extent)
-    needed = (query_pos[count - 1] + window) // window
-    initial = (
-        jnp.zeros((count, kv_local, per_key, HEAD), jnp.float32),
-        jnp.zeros((count, kv_local, per_key), jnp.float32),
-    )
-
-    def visit(step_index, carried):
-        first_key = (needed - 1 - step_index) * window
-        key_block = lax.dynamic_slice_in_dim(key_all, first_key, window, 0).reshape(
-            window, kv_local, HEAD
+LOG2E = 1.4426950408889634
+KEY_BLOCK = 256
+ROWS = 128
+
+
+def attention_kernel(place_ref, bias_ref, query_ref, kv_ref, out_ref, stacked, outputs, used):
+    place = place_ref[0]
+    heads = query_ref.shape[1] // HEAD
+    rows = query_ref.shape[0]
+    for head in range(heads):
+        stacked[head * rows : (head + 1) * rows] = query_ref[:, head * HEAD : (head + 1) * HEAD]
+    outputs[...] = jnp.zeros_like(outputs)
+    used[...] = jnp.zeros_like(used)
+    later = (
+        lax.broadcasted_iota(jnp.int32, (KEY_BLOCK, KEY_BLOCK), 0)
+        > lax.broadcasted_iota(jnp.int32, (KEY_BLOCK, KEY_BLOCK), 1)
+    ).astype(jnp.float32).astype(jnp.bfloat16)
+    factor = HEAD ** (-0.5) * LOG2E
+    needed = (place * rows + rows + KEY_BLOCK - 1) // KEY_BLOCK
+
+    def visit(block, masked):
+        keys = kv_ref[pl.ds(pl.multiple_of(block * KEY_BLOCK, KEY_BLOCK), KEY_BLOCK), :HEAD]
+        values = kv_ref[pl.ds(pl.multiple_of(block * KEY_BLOCK, KEY_BLOCK), KEY_BLOCK), HEAD:]
+        scores = lax.dot_general(
+            stacked[...], keys, (((1,), (1,)), ((), ())), preferred_element_type=jnp.float32
         )
-        value_block = lax.dynamic_slice_in_dim(value_all, first_key, window, 0).reshape(
-            window, kv_local, HEAD
+        breaks, leads = [], []
+        if masked:
+            query_pos = place * rows + lax.broadcasted_iota(jnp.int32, (rows, KEY_BLOCK), 0)
+            key_pos = block * KEY_BLOCK + lax.broadcasted_iota(jnp.int32, (rows, KEY_BLOCK), 1)
+            before = key_pos < query_pos
+        for head in range(heads):
+            z = scores[head * rows : (head + 1) * rows] * factor + bias_ref[head] * LOG2E
+            log_term = jnp.log2(1.0 + jnp.exp2(-jnp.abs(z)))
+            softplus = jnp.maximum(z, 0.0) + log_term
+            if masked:
+                softplus = jnp.where(before, softplus, 0.0)
+            breaks.append(softplus)
+            leads.append(jnp.minimum(z, 0.0) - log_term)
+        behind = jnp.dot(
+            jnp.concatenate([b.astype(jnp.bfloat16) for b in breaks], axis=0),
+            later,
+            preferred_element_type=jnp.float32,
         )
-        key_pos = first_key + jnp.arange(window, dtype=jnp.int32)
-        return stick_block(
-            carried, query_rows, key_block, value_block, head_bias, query_pos, key_pos
+        weights = []
+        for head in range(heads):
+            at = slice(head * rows, (head + 1) * rows)
+            past = behind[at]
+            gone = used[at]
+            weight = jnp.exp2(leads[head] - past - jnp.concatenate([gone, gone], axis=1))
+            if masked:
+                weight = jnp.where(before, weight, 0.0)
+            weights.append(weight.astype(jnp.bfloat16))
+            used[at] = gone + jnp.broadcast_to(past[:, :1] + breaks[head][:, :1], gone.shape)
+        outputs[...] += jnp.dot(
+            jnp.concatenate(weights, axis=0), values, preferred_element_type=jnp.float32
         )
 
-    return lax.fori_loop(0, needed, visit, initial)[0]
-
-
-def normed_heads(output):
-    scaled = output * lax.rsqrt(jnp.mean(output * output, axis=-1, keepdims=True) + epsilon)
-    return scaled.astype(jnp.bfloat16).reshape(output.shape[0], -1)
+    visit(needed - 1, True)
+
+    def step(index, carried):
+        visit(needed - 2 - index, False)
+        return carried
+
+    lax.fori_loop(0, needed - 1, step, 0)
+    for head in range(heads):
+        output = outputs[head * rows : (head + 1) * rows]
+        scaled = output * lax.rsqrt(jnp.mean(output * output, axis=-1, keepdims=True) + epsilon)
+        out_ref[:, head * HEAD : (head + 1) * HEAD] = scaled.astype(jnp.bfloat16)
+
+
+def attend(queries, key_values, break_bias, position):
+    rows, width = queries.shape
+    stack = rows * (width // HEAD)
+    return pl.pallas_call(
+        attention_kernel,
+        name="stick_attention",
+        out_shape=jax.ShapeDtypeStruct((rows, width), jnp.bfloat16),
+        in_specs=[
+            pl.BlockSpec(memory_space=pltpu.SMEM),
+            pl.BlockSpec(memory_space=pltpu.SMEM),
+            pl.BlockSpec(memory_space=pltpu.VMEM),
+            pl.BlockSpec(memory_space=pltpu.VMEM),
+        ],
+        out_specs=pl.BlockSpec(memory_space=pltpu.VMEM),
+        scratch_shapes=[
+            pltpu.VMEM((stack, HEAD), jnp.bfloat16),
+            pltpu.VMEM((stack, HEAD), jnp.float32),
+            pltpu.VMEM((stack, HEAD), jnp.float32),
+        ],
+        compiler_params=pltpu.CompilerParams(vmem_limit_bytes=40 * 1024 * 1024),
+    )(position, break_bias, queries, key_values)
 
 
 def on_device(
@@ -94,15 +133,10 @@
     out_gain,
 ):
     length = queries.shape[0]
-    kv_local = keys.shape[1] // HEAD
-    per_key = queries.shape[1] // keys.shape[1]
-    query_rows = queries.reshape(length, kv_local, per_key, HEAD)
-    head_bias = break_bias.reshape(kv_local, per_key)
     position = lax.axis_index("sp")
-    offset = position * length
-    query_pos = offset + jnp.arange(length, dtype=jnp.int32)
-    key_all, value_all = sent_together((keys, values), "sp", 0, 1)
-    head_out = normed_heads(attend_all(query_rows, query_pos, key_all, value_all, head_bias))
+    own = jnp.concatenate([keys, values], axis=1)
+    key_values = lax.all_gather(own, "sp", axis=0, tiled=True)
+    head_out = attend(queries, key_values, break_bias, position.reshape(1).astype(jnp.int32))
     quarters = lax.axis_size("tp")
     quarter = lax.axis_index("tp")
     slice_rows = length // quarters

time: 568 us -> 370 us (0.65)
  blocking collectives: 288 us -> 105 us
  other arithmetic: 30.3 us -> 21.5 us
  matrix products: 21.4 us -> 15.1 us
    all_to_all x1, blocking collectives: 235 us -> 51.9 us  [on_device(): lax.all_to_all(outgoing, 'sp', split_axis=1, concat_axis=1, tiled=True)]
    another operation x2 -> x0, other arithmetic: 5.91 us -> none
where the time goes in v1:
time: 370 us; the launch traced here: 369 us
  waiting for transfers between devices  171 us (46%)
  blocking collectives  105 us (28%)
  local copies, waits for them, and re-layouts  24.8 us (7%)
  other arithmetic  21.5 us (6%)
  starting transfers between devices  16.1 us (4%)
  matrix products  15.1 us (4%)
  between operations  13.6 us (4%)
    all_gather x1, waiting for transfers between devices, on_device(): key_values = lax.all_gather(own, 'sp', axis=0, tiled=True)  83.8 us
    all_to_all x1, blocking collectives, summed_on_arrival(): lax.all_to_all(parts, axis, split_axis=0, concat_axis=0, tiled=True)  53.5 us
    all_to_all x1, blocking collectives, on_device(): lax.all_to_all(outgoing, 'sp', split_axis=1, concat_axis=1, tiled=True)  51.9 us
    all_gather x1, waiting for transfers between devices, on_device(): piece = lax.all_gather(arrived, 'tp', axis=0, tiled=True)  45.8 us
    all_to_all x1, waiting for transfers between devices, on_device(): lax.all_to_all(results, 'sp', split_axis=0, concat_axis=0, tiled=True)  27.8 us
    all_to_all x1, waiting for transfers between devices, summed_on_arrival(): lax.all_to_all(parts, axis, split_axis=0, concat_axis=0, tiled=True)  14 us
    all_to_all x1, starting transfers between devices, on_device(): lax.all_to_all(results, 'sp', split_axis=0, concat_axis=0, tiled=True)  12.1 us
    unnamed x24, local copies, waits for them, and re-layouts  10.6 us
  transfers between devices with their start and end apart: 4, of which 4 were waited for; matrix products, arithmetic and copies ran while one was open for 1% of the time, Pallas kernels for 0%

profile of v1, /device:TPU:1, one launch (start us, length us, event | category | flops | bytes accessed | tf_op | source)
XLA Modules:
  0.0 369.5 jit_solution(290426765756618685)
XLA Ops:
  6.5 1.6 pad_maximum_fusion
  9.5 83.8 %all-gather.4.cloned.1.call-done.kv_ref = bf16[8192,256]{1,0:T(8,128)(2,1)} async-done(((bf16[128,256]{1,0:T(8,128)(2,1)}), bf16[8192,256]{1,0:T(8,128)(2,1)}) %all-gather.4.cloned.1.call-update) | async-done | bytes 4194320 | tf_op jit(solution)/shard_map/all_gather | solution.py:138
  93.3 2.2 copy-done.1
  99.2 1.7 convolution_convert_fusion.1
  101.0 4.0 %all-to-all-start = ((bf16[4,32,4096]{2,1,0:T(8,128)(2,1)}), bf16[4,32,4096]{2,1,0:T(8,128)(2,1)S(1)}, u32[]{:S(2)}, u32[]{:S(2)}) async-start(bf16[4,32,4096]{2,1,0:T(8,128)(2,1)} %bitcast.47), calls=%async_computation | async-start | bytes 2097152 | tf_op jit(solution)/shard_map/all_to_all | solution.py:22
  105.6 14.0 %all-to-all-done = bf16[4,32,4096]{2,1,0:T(8,128)(2,1)S(1)} async-done(((bf16[4,32,4096]{2,1,0:T(8,128)(2,1)}), bf16[4,32,4096]{2,1,0:T(8,128)(2,1)S(1)}, u32[]{:S(2)}, u32[]{:S(2)}) %all-to-all-start) | async-done | bytes 1048608 | tf_op jit(solution)/shard_map/all_to_all | solution.py:22
  120.9 1.4 scatter_custom_fusion
  122.3 1.8 scatter_custom_fusion.1
  124.2 3.7 %copy.54 = bf16[1,128,4096]{2,0,1:T(2,128)(2,1)} copy(bf16[1,128,4096]{2,1,0:T(8,128)(2,1)S(1)} %bitcast.45) | data formatting | bytes 2097152 | tf_op jit(solution)/shard_map/scatter | solution.py:168
  128.4 8.4 %reduce.10 = bf16[128,4096]{1,0:T(8,128)(2,1)S(1)} reduce(bf16[128,1,4096]{2,1,0:T(2,128)(2,1)} %bitcast.44, bf16[]{:T(256)} %broadcast.163), dimensions={1}, to_apply=%bitcast.40.reduce_sub_computation | reduce | bytes 2097154
  136.8 1.5 reshape.213
  138.3 51.9 %all_to_all.27 = bf16[64,2,4096]{2,1,0:T(2,128)(2,1)S(1)} all-to-all(bf16[64,2,4096]{2,1,0:T(2,128)(2,1)} %reshape.213), channel_id=1, replica_groups=mesh['sp'=64,'tp'=4] {'sp'}, dimensions={0} | all-to-all | bytes 2097152 | tf_op jit(solution)/shard_map/all_to_all | solution.py:169
  190.2 3.5 reshape.214
  193.7 3.7 %copy.47 = bf16[1,128,4096]{2,1,0:T(8,128)(2,1)} copy(bf16[1,128,4096]{2,0,1:T(2,128)(2,1)} %bitcast.43) | data formatting | bytes 2097152 | tf_op jit(solution)/shard_map/all_to_all | solution.py:169
  197.4 45.8 %all-gather.6.cloned.1.call-done = bf16[1,512,4096]{2,1,0:T(8,128)(2,1)} async-done(((bf16[1,128,4096]{2,1,0:T(8,128)(2,1)}), bf16[1,512,4096]{2,1,0:T(8,128)(2,1)}) %all-gather.6.cloned.1.call-update) | async-done | bytes 4194320 | tf_op jit(solution)/shard_map/all_gather | solution.py:172
  243.3 4.1 %fusion.2 = f32[512,256]{1,0:T(8,128)S(1)} fusion(bf16[1,512,4096]{2,1,0:T(8,128)(2,1)} %all-gather.6.cloned.1.call-done, bf16[1,4096,256]{2,1,0:T(8,128)(2,1)} %param.22), kind=kOutput, calls=%fused_computation.8 | convolution fusion | flops 1073741824 | bytes 6815744 | tf_op jit(solution)/shard_map/dot_general | solution.py:173
  247.4 9.3 %convolution_convert_fusion = bf16[512,4096]{1,0:T(8,128)(2,1)} fusion(bf16[1,256,4096]{2,1,0:T(8,128)(2,1)S(1)} %copy-done, bf16[1,4096,256]{2,1,0:T(8,128)(2,1)} %param.23, bf16[1,512,4096]{2,1,0:T(8,128)(2,1)} %all-gather.6.cloned.1.call-done, f32[512,256]{1,0:T(8,128)S(1)} %fusion.2), kind=kOutput, calls=%fused_computation.4 | convolution fusion | flops 2150367232 | bytes 13107200 | tf_op jit(solution)/shard_map/dot_general | solution.py:178
  256.7 53.5 %all_to_all.28 = bf16[4,128,4096]{2,1,0:T(8,128)(2,1)} all-to-all(bf16[4,128,4096]{2,1,0:T(8,128)(2,1)} %bitcast.46), channel_id=1, replica_groups=mesh['sp'=64,'tp'=4] {'tp'}, dimensions={0} | all-to-all | bytes 8388608 | tf_op jit(solution)/shard_map/all_to_all | solution.py:22
  310.3 3.1 reduce_sum.54
  313.3 1.5 all_to_all.20
  314.8 12.1 %all-to-all-start.3 = ((bf16[64,2,4096]{2,1,0:T(2,128)(2,1)}), bf16[64,2,4096]{2,1,0:T(2,128)(2,1)}, u32[]{:S(2)}, u32[]{:S(2)}) async-start(bf16[64,2,4096]{2,1,0:T(2,128)(2,1)} %all_to_all.20), calls=%async_computation.3 | async-start | bytes 2097152 | tf_op jit(solution)/shard_map/all_to_all | solution.py:180
  327.2 27.8 %all-to-all-done.3 = bf16[64,2,4096]{2,1,0:T(2,128)(2,1)} async-done(((bf16[64,2,4096]{2,1,0:T(2,128)(2,1)}), bf16[64,2,4096]{2,1,0:T(2,128)(2,1)}, u32[]{:S(2)}, u32[]{:S(2)}) %all-to-all-start.3) | async-done | bytes 1048608 | tf_op jit(solution)/shard_map/all_to_all | solution.py:180
  355.0 1.5 all_to_all.22
  360.6 2.0 fusion.24
  (48 shorter events, 11.9 us)
Async XLA Ops:
  6.5 240.9 %copy-start = (bf16[1,256,4096]{2,1,0:T(8,128)(2,1)S(1)}, bf16[1,256,4096]{2,1,0:T(8,128)(2,1)}, u32[]{:S(2)}) copy-start(bf16[1,256,4096]{2,1,0:T(8,128)(2,1)} %param.24) | copy-start | bytes 6291460
  6.5 86.8 %all-gather.4.cloned.1.call-start = ((), (), s32[]{:S(2)}) async-start(), calls=%async_computation.4 | async-start | bytes 4259840 | tf_op jit(solution)/shard_map/all_gather | solution.py:138
  93.3 2.2 copy-start.1
  95.5 0.9 copy-start.2
  96.4 0.7 copy-start.3
  97.1 2.2 copy-start.4
  99.2 21.7 %copy-start.5 = (f32[4096]{0:T(1024)S(1)}, f32[4096]{0:T(1024)}, u32[]{:S(2)}) copy-start(f32[4096]{0:T(1024)} %param.19) | copy-start | bytes 49156
  101.0 18.6 %all-to-all-start = ((bf16[4,32,4096]{2,1,0:T(8,128)(2,1)}), bf16[4,32,4096]{2,1,0:T(8,128)(2,1)S(1)}, u32[]{:S(2)}, u32[]{:S(2)}) async-start(bf16[4,32,4096]{2,1,0:T(8,128)(2,1)} %bitcast.47), calls=%async_computation | async-start | bytes 2097152 | tf_op jit(solution)/shard_map/all_to_all | solution.py:22
  105.0 138.3 %all-gather.6.cloned.1.call-start = ((), (), s32[]{:S(2)}) async-start(), calls=%async_computation.5 | async-start | bytes 5242880 | tf_op jit(solution)/shard_map/all_gather | solution.py:172
  310.2 16.7 %copy-start.7 = (f32[128]{0:T(128)S(1)}, f32[128]{0:T(128)}, u32[]{:S(2)}) copy-start(f32[128]{0:T(128)} %param.21) | copy-start | bytes 1540
  314.8 40.2 %all-to-all-start.3 = ((bf16[64,2,4096]{2,1,0:T(2,128)(2,1)}), bf16[64,2,4096]{2,1,0:T(2,128)(2,1)}, u32[]{:S(2)}, u32[]{:S(2)}) async-start(bf16[64,2,4096]{2,1,0:T(2,128)(2,1)} %all_to_all.20), calls=%async_computation.3 | async-start | bytes 2097152 | tf_op jit(solution)/shard_map/all_to_all | solution.py:180
  326.9 33.7 %copy-start.6 = (f32[4096]{0:T(1024)S(1)}, f32[4096]{0:T(1024)}, u32[]{:S(2)}) copy-start(f32[4096]{0:T(1024)} %param.25) | copy-start | bytes 49156
Sparse Core Ops, SparseCore 0:
  10.1 83.1 all-gather.3
  197.6 45.6 all-gather.5
